TPU v7x, 32 devices: a whole 2x2x4 slice. The times are simulated.
32 devices in a mesh: sp: 8 (over z, y), tp: 4 (over x, core).
Axes of the slice: x: 2, y: 2, z: 4, core: 2. Of those that a mesh axis runs over, the one named last changes fastest.
Arguments:
- skip_stream: bfloat16 [2048, 2048], P('sp', 'tp'), may hold values from -20 to 20
- narrow_lookup_matrix: bfloat16 [2048, 256], P('sp', 'tp'), may hold values from -6 to 6
- narrow_probe_matrix: bfloat16 [2048, 256], P('sp', 'tp'), may hold values from -6 to 6
- narrow_retention_logits: bfloat16 [2048, 256], P('sp', 'tp'), may hold values from -6 to 16
- broad_lookup_matrix: bfloat16 [2048, 512], P('sp', 'tp'), may hold values from -6 to 6
- broad_probe_matrix: bfloat16 [2048, 512], P('sp', 'tp'), may hold values from -6 to 6
- broad_retention_logits: bfloat16 [2048, 512], P('sp', 'tp'), may hold values from -6 to 16
- content_vectors: bfloat16 [2048, 4, 2, 128], P('sp', 'tp'), may hold values from -6 to 6
- extra_log_retention: float32 [2048, 2, 4], P('sp', None, 'tp'), may hold values from -0.7 to 0
- per_branch_scaling: bfloat16 [4, 2, 128], P('tp'), may hold values from 0.099609375 to 1.8984375
- final_projection_matrix: bfloat16 [1024, 2048], P(None, 'tp'), may hold values from -0.1875 to 0.1875
- channel_blend_scaling: bfloat16 [2048], replicated, may hold values from 0.099609375 to 1.8984375
- switch_expansion_matrix: bfloat16 [2048, 5632], P('sp', 'tp'), may hold values from -0.125 to 0.125
- content_expansion_matrix: bfloat16 [2048, 5632], P('sp', 'tp'), may hold values from -0.125 to 0.125
- convolution_kernel: bfloat16 [3, 2, 5632], P(None, None, 'tp'), may hold values from -3.5 to 3.5
- contraction_matrix: bfloat16 [5632, 2048], P('tp', 'sp'), may hold values from -0.078125 to 0.078125
Outputs:
- mixed: bfloat16 [2048, 2048], P('sp', 'tp')
All inputs are finite; a program needn't handle non-finite values.
Results may differ from a plain program's by a relative error of at most 0.011.
Values may be sent and summed in bfloat16 or wider, within the bound.
A program may use at most 64 MiB of HBM per device.

v0:
```python
import jax
import jax.numpy as jnp
from jax import lax
from jax.sharding import PartitionSpec as P

BLOCK = 64
EPSILON = 1e-06
SOFTENING = 16.0
HIGHEST = lax.Precision.HIGHEST


def entering(value, axis, combine, identity):
    devices, mine = (lax.axis_size(axis), lax.axis_index(axis))
    everything = jax.tree.map(
        lambda part, kind: lax.all_gather(part.astype(kind), axis),
        value,
        jax.tree.map(lambda a: jnp.bfloat16 if a.dtype == jnp.float32 else a.dtype, value),
    )
    start = jax.tree.map(
        lambda part, zero: jnp.broadcast_to(jnp.asarray(zero, part.dtype), part.shape),
        value,
        identity,
    )

    def turn(k, before):
        reached = k < mine
        new = combine(
            before, jax.tree.map(lambda part, own: part[k].astype(own.dtype), everything, value)
        )
        return jax.tree.map(lambda a, b: jnp.where(reached, a, b), new, before)

    return lax.fori_loop(0, devices, turn, start)


def shifted(value, axis, steps):
    count = lax.axis_size(axis)
    initial, last = (max(0, -steps), min(count, count - steps))
    return lax.ppermute(value, axis, [(source, source + steps) for source in range(initial, last)])


def blocked(array):
    return array.reshape(array.shape[0] // BLOCK, BLOCK, array.shape[1], array.shape[2]).transpose(
        0, 2, 1, 3
    )


def group_parts(query_rows, input_keys, values_in, log_decay):
    query_blocks = blocked(query_rows)
    key_blocks = blocked(input_keys)
    value_blocks = blocked(values_in)
    inner = jnp.cumsum(blocked(log_decay), axis=2)
    last = inner[:, :, -1:, :]
    middle = inner[:, :, BLOCK // 2 - 1 : BLOCK // 2, :]
    scores = jnp.einsum(
        "nhid,nhjd->nhij",
        query_blocks * jnp.exp(inner - middle),
        key_blocks * jnp.exp(middle - inner),
        precision=HIGHEST,
    )
    lower = jnp.tril(jnp.ones((BLOCK, BLOCK), dtype=bool))
    local_out = jnp.einsum(
        "nhij,nhjv->nhiv", jnp.where(lower, scores, 0.0), value_blocks, precision=HIGHEST
    )
    query_carry = query_blocks * jnp.exp(inner)
    key_carry = key_blocks * jnp.exp(last - inner)
    block_logs = last[:, :, 0, :]
    fade = jnp.exp(block_logs)
    totals = jnp.sum(block_logs, axis=0)
    after = totals[None] - jnp.cumsum(block_logs, axis=0)
    summary = jnp.einsum(
        "nhjd,nhjv->hdv", key_carry * jnp.exp(after)[:, :, None, :], value_blocks, precision=HIGHEST
    )
    return ((local_out, query_carry, key_carry, value_blocks, fade), (jnp.exp(totals), summary))


def group_finish(parts, incoming):
    local_out, query_carry, key_carry, value_blocks, fade = parts

    def advance(state, inputs):
        query_part, key_part, value_part, fade_part = inputs
        output = jnp.einsum("hid,hdv->hiv", query_part, state, precision=HIGHEST)
        state = fade_part[..., None] * state + jnp.einsum(
            "hjd,hjv->hdv", key_part, value_part, precision=HIGHEST
        )
        return (state, output)

    _, carried = lax.scan(advance, incoming, (query_carry, key_carry, value_blocks, fade))
    total = local_out + carried
    return total.transpose(0, 2, 1, 3).reshape(-1, total.shape[1], total.shape[3])


def head_norm(output, gain):
    scale = lax.rsqrt(jnp.mean(output * output, axis=-1, keepdims=True) + EPSILON)
    return output * scale * gain.astype(jnp.float32)


def chain(earlier, later):
    joined = []
    for (fade_early, state_early), (fade_late, state_late) in zip(earlier, later):
        joined.append((fade_early * fade_late, fade_late[..., None] * state_early + state_late))
    return tuple(joined)


def convolve(upward, tap_rows):
    return tap_rows[0] * upward[:-2] + tap_rows[1] * upward[1:-1] + tap_rows[2] * upward[2:]


def local(
    skip_stream,
    narrow_lookup_matrix,
    narrow_probe_matrix,
    narrow_retention_logits,
    broad_lookup_matrix,
    broad_probe_matrix,
    broad_retention_logits,
    content_vectors,
    extra_log_retention,
    per_branch_scaling,
    final_projection_matrix,
    channel_blend_scaling,
    switch_expansion_matrix,
    content_expansion_matrix,
    convolution_kernel,
    contraction_matrix,
):
    item_count = skip_stream.shape[0]
    heads = content_vectors.shape[1]
    value_data = content_vectors.astype(jnp.float32)

    def build_arguments(query_rows, input_keys, forget_gates, spike_column):
        model_width = forget_gates.shape[1] // heads
        query_data = query_rows.astype(jnp.float32).reshape(
            item_count, heads, model_width
        ) * model_width ** (-0.5)
        key_data = input_keys.astype(jnp.float32).reshape(item_count, heads, model_width)
        decay_factor = (
            jax.nn.log_sigmoid(
                forget_gates.astype(jnp.float32).reshape(item_count, heads, model_width)
            )
            / SOFTENING
            + spike_column[:, :, None]
        )
        return (query_data, key_data, decay_factor)

    narrow_lookup_vector, narrow_probe_vector, narrow_probe_dim = build_arguments(
        narrow_lookup_matrix,
        narrow_probe_matrix,
        narrow_retention_logits,
        extra_log_retention[:, 0],
    )
    broad_lookup_vector, broad_probe_vector, broad_probe_dim = build_arguments(
        broad_lookup_matrix, broad_probe_matrix, broad_retention_logits, extra_log_retention[:, 1]
    )
    parts_small, summary_small = group_parts(
        narrow_lookup_vector, narrow_probe_vector, value_data[:, :, 0], narrow_probe_dim
    )
    parts_large, summary_large = group_parts(
        broad_lookup_vector, broad_probe_vector, value_data[:, :, 1], broad_probe_dim
    )
    identity = (
        (jnp.ones_like(summary_small[0]), jnp.zeros_like(summary_small[1])),
        (jnp.ones_like(summary_large[0]), jnp.zeros_like(summary_large[1])),
    )
    incoming = entering((summary_small, summary_large), "sp", chain, identity)
    out_small = group_finish(parts_small, incoming[0][1])
    out_large = group_finish(parts_large, incoming[1][1])
    stacked = jnp.stack(
        [
            head_norm(out_small, per_branch_scaling[:, 0]),
            head_norm(out_large, per_branch_scaling[:, 1]),
        ],
        axis=2,
    )
    heads_in = stacked.reshape(item_count, -1).astype(jnp.bfloat16)
    projected = jnp.dot(
        lax.all_gather(heads_in, "tp", axis=1, tiled=True),
        final_projection_matrix,
        preferred_element_type=jnp.float32,
    )
    resid_data = (
        (skip_stream.astype(jnp.float32) + projected).astype(jnp.bfloat16).astype(jnp.float32)
    )
    resid = resid_data.astype(jnp.bfloat16)
    whole = lax.all_gather(resid, "tp", axis=1, tiled=True).astype(jnp.float32)
    scale = lax.rsqrt(jnp.mean(whole * whole, axis=1, keepdims=True) + EPSILON)
    normed = (whole * scale * channel_blend_scaling.astype(jnp.float32)).astype(jnp.bfloat16)
    gate_rows, value_rows = (
        lax.all_gather(switch_expansion_matrix, "sp", axis=0, tiled=True),
        lax.all_gather(content_expansion_matrix, "sp", axis=0, tiled=True),
    )
    up_gate = jnp.dot(normed, gate_rows, preferred_element_type=jnp.float32).astype(jnp.bfloat16)
    up_value = jnp.dot(normed, value_rows, preferred_element_type=jnp.float32).astype(jnp.bfloat16)
    earlier_rows = shifted((up_value[-2:], up_gate[-2:]), "sp", 1)
    taps = convolution_kernel.astype(jnp.float32)
    value_ext = jnp.concatenate([earlier_rows[0], up_value], axis=0).astype(jnp.float32)
    gate_ext = jnp.concatenate([earlier_rows[1], up_gate], axis=0).astype(jnp.float32)
    conv_value = convolve(value_ext, taps[:, 0])
    conv_gate = convolve(gate_ext, taps[:, 1])
    hidden = (jax.nn.silu(conv_gate) * conv_value).astype(jnp.bfloat16)
    terms = jnp.dot(
        hidden,
        lax.all_gather(contraction_matrix, "sp", axis=1, tiled=True),
        preferred_element_type=jnp.float32,
    )
    down = lax.psum_scatter(
        terms.astype(jnp.bfloat16), "tp", scatter_dimension=1, tiled=True
    ).astype(jnp.float32)
    return (resid_data + down).astype(jnp.bfloat16)


def solution(mesh):
    in_specs = (
        P("sp", "tp"),
        P("sp", "tp"),
        P("sp", "tp"),
        P("sp", "tp"),
        P("sp", "tp"),
        P("sp", "tp"),
        P("sp", "tp"),
        P("sp", "tp", None, None),
        P("sp", None, "tp"),
        P("tp", None, None),
        P(None, "tp"),
        P(),
        P("sp", "tp"),
        P("sp", "tp"),
        P(None, None, "tp"),
        P("tp", "sp"),
    )
    out_specs = P("sp", "tp")
    return jax.shard_map(local, mesh=mesh, in_specs=in_specs, out_specs=out_specs, check_vma=False)
```

profile of v0, /device:TPU:0, one launch (start us, length us, event | category | flops | bytes accessed | tf_op | source)
XLA Modules:
  0.0 465.0 jit_solution(4777201416008957610)
XLA Ops:
  6.6 1.3 fusion.88
  7.9 1.2 fusion.87
  9.1 0.7 fusion.89
  9.8 1.0 fusion.56
  11.0 0.3 fusion.42
  11.3 32.6 %all-gather.3 = bf16[1024,128]{1,0:T(8,128)(2,1)S(1)} all-gather(bf16[128,128]{1,0:T(8,128)(2,1)S(1)} %fusion.42), channel_id=5, replica_groups=mesh['sp'=8,'tp'=4] {'sp'}, dimensions={0}, use_global_device_ids=true | all-gather | bytes 294912 | tf_op jit(solution)/shard_map/all_gather | solution.py:15
  44.4 0.3 fusion.43
  44.7 30.5 %all-gather.1 = bf16[512,128]{1,0:T(8,128)(2,1)S(1)} all-gather(bf16[64,128]{1,0:T(8,128)(2,1)S(1)} %fusion.43), channel_id=3, replica_groups=mesh['sp'=8,'tp'=4] {'sp'}, dimensions={0}, use_global_device_ids=true | all-gather | bytes 147456 | tf_op jit(solution)/shard_map/all_gather | solution.py:15
  75.2 0.6 dynamic-slice
  76.4 0.2 dynamic-update-slice
  76.6 21.4 %all-reduce = bf16[512]{0:T(512)(128)(2,1)S(1)} all-reduce(bf16[512]{0:T(512)(128)(2,1)S(1)} %dynamic-update-slice), channel_id=2, replica_groups=mesh['sp'=8,'tp'=4] {'sp'}, use_global_device_ids=true, to_apply=%add | all-reduce | flops 512 | bytes 2048
  98.1 16.3 %all-gather.4 = bf16[8,1,128]{2,1,0:T(2,128)(2,1)S(1)} all-gather(bf16[1,1,128]{2,1,0:T(2,128)(2,1)S(1)} %convert_bitcast_fusion), channel_id=4, replica_groups=mesh['sp'=8,'tp'=4] {'sp'}, dimensions={0}, use_global_device_ids=true | all-gather | bytes 2304 | tf_op jit(solution)/shard_map/all_gather | solution.py:15
  114.4 1.6 while.42
  116.2 1.8 while.40
  116.4 0.2 fusion.124
  116.9 0.2 fusion.124
  117.4 0.2 fusion.124
  117.8 0.2 fusion.124
  118.1 0.4 convolution_select_fusion.1
  118.4 0.3 multiply_reduce_fusion.1
  119.0 2.1 while.41
  119.3 0.3 fusion.131
  119.8 0.3 fusion.131
  120.1 0.2 fusion.132
  120.3 0.3 fusion.131
  120.9 0.3 fusion.131
  121.2 0.4 convolution_select_fusion
  121.6 0.3 multiply_reduce_fusion
  122.2 7.2 %all_gather.41 = bf16[256,1024]{0,1:T(8,128)(2,1)S(1)} all-gather(bf16[256,256]{0,1:T(8,128)(2,1)S(1)} %bitcast.236), channel_id=1, replica_groups=mesh['sp'=8,'tp'=4] {'tp'}, dimensions={1}, use_global_device_ids=true | all-gather | bytes 655360 | tf_op jit(solution)/shard_map/all_gather | solution.py:176
  129.4 1.2 fusion.39
  130.6 0.7 all-gather.12.cloned.1.call-update
  131.4 0.7 all-gather.14.cloned.1.call-update
  132.1 0.5 all-gather.16.cloned.1.call-update
  132.9 12.6 %all-gather.10.cloned.1.call-done = bf16[256,2048]{1,0:T(8,128)(2,1)} async-done(((bf16[256,512]{1,0:T(8,128)(2,1)}), bf16[256,2048]{1,0:T(8,128)(2,1)}) %all-gather.10.cloned.1.call-update) | async-done | bytes 1048592 | tf_op jit(solution)/shard_map/all_gather | solution.py:184
  145.5 1.5 fusion.30
  147.0 93.0 %all-gather.12.cloned.1.call-done = bf16[2048,1408]{1,0:T(8,128)(2,1)} async-done(((bf16[256,1408]{1,0:T(8,128)(2,1)}), bf16[2048,1408]{1,0:T(8,128)(2,1)}) %all-gather.12.cloned.1.call-update) | async-done | bytes 5767184 | tf_op jit(solution)/shard_map/all_gather | solution.py:188
  240.0 4.8 %convolution_convert_fusion.1 = bf16[256,1408]{1,0:T(8,128)(2,1)S(1)} fusion(bf16[2048,1408]{1,0:T(8,128)(2,1)} %all-gather.12.cloned.1.call-done, bf16[256,2048]{1,0:T(8,128)(2,1)} %all-gather.10.cloned.1.call-done, f32[2048]{0:T(1024)S(1)} %convert_element_type.216, f32[256]{0:T(256)S(1)} %add_rsqrt_fusion.2), kind=kOutput, calls=%fused_computation.43 | convolution fusion | flops 1478852608 | bytes 7545856 | tf_op jit(solution)/shard_map/dot_general | solution.py:191
  244.8 0.9 copy-done.3
  245.7 2.5 collective-permute-start
  248.2 84.5 %all-gather.14.cloned.1.call-done = bf16[2048,1408]{1,0:T(8,128)(2,1)} async-done(((bf16[256,1408]{1,0:T(8,128)(2,1)}), bf16[2048,1408]{1,0:T(8,128)(2,1)}) %all-gather.14.cloned.1.call-update) | async-done | bytes 5767184 | tf_op jit(solution)/shard_map/all_gather | solution.py:189
  332.7 4.6 convolution_convert_fusion
  337.3 2.5 collective-permute-start.1
  339.9 1.1 collective-permute-done.1
  341.1 1.3 maximum_convert_fusion.1
  342.4 83.6 %all-gather.16.cloned.1.call-done = bf16[1408,2048]{1,0:T(8,128)(2,1)} async-done(((bf16[1408,256]{1,0:T(8,128)(2,1)}), bf16[1408,2048]{1,0:T(8,128)(2,1)}) %all-gather.16.cloned.1.call-update) | async-done | bytes 5767184 | tf_op jit(solution)/shard_map/all_gather | solution.py:202
  426.0 7.6 %convolution_convert_fusion.2 = bf16[256,2048]{1,0:T(8,128)(2,1)} fusion(bf16[1408,2048]{1,0:T(8,128)(2,1)} %all-gather.16.cloned.1.call-done, f32[258,1408]{1,0:T(8,128)} %maximum_convert_fusion.1, f32[258,1408]{1,0:T(8,128)S(1)} %maximum_convert_fusion, f32[1408]{0:T(1024)S(1)} %get-tuple-element.317, f32[1408]{0:T(1024)S(1)} %get-tuple-element.318, ...), kind=kOutput, calls=%fused_computation.44 | convolution fusion | flops 1482686464 | bytes 15515648 | tf_op jit(solution)/shard_map/dot_general | solution.py:200
  433.6 23.1 %reduce-scatter.2.cloned.1.call-done = bf16[256,512]{1,0:T(8,128)(2,1)} async-done(((bf16[256,2048]{1,0:T(8,128)(2,1)}), bf16[256,512]{1,0:T(8,128)(2,1)}) %reduce-scatter.2.cloned.1.call-update) | async-done | bytes 262160 | tf_op jit(solution)/shard_map/reduce_scatter | solution.py:205
  456.8 1.7 add_convert_fusion
  (128 shorter events, 4.9 us)
Async XLA Ops:
  6.5 122.9 %copy-start = (bf16[1024,512]{1,0:T(8,128)(2,1)S(1)}, bf16[1024,512]{1,0:T(8,128)(2,1)}, u32[]{:S(2)}) copy-start(bf16[1024,512]{1,0:T(8,128)(2,1)} %param.32) | copy-start | bytes 3145732
  6.5 4.5 copy-start.5
  6.5 37.4 %copy-start.7 = (bf16[256,64]{0,1:T(8,128)(2,1)S(1)}, bf16[256,64]{0,1:T(8,128)(2,1)}, u32[]{:S(2)}) copy-start(bf16[256,64]{0,1:T(8,128)(2,1)} %param.25) | copy-start | bytes 98308
  6.5 138.9 %all-gather.10.cloned.1.call-start = ((), (), s32[]{:S(2)}) async-start(), calls=%async_computation.1 | async-start | bytes 1310720 | tf_op jit(solution)/shard_map/all_gather | solution.py:184
  7.9 36.4 %copy-start.8 = (bf16[256,64]{0,1:T(8,128)(2,1)S(1)}, bf16[256,64]{0,1:T(8,128)(2,1)}, u32[]{:S(2)}) copy-start(bf16[256,64]{0,1:T(8,128)(2,1)} %param.24) | copy-start | bytes 98308
  9.8 65.4 %copy-start.14 = (u32[32]{0:T(128)S(1)}, u32[32]{0:T(128)}, u32[]{:S(2)}) copy-start(u32[32]{0:T(128)} %constant.109) | copy-start | bytes 388
  43.9 72.1 %copy-start.9 = (bf16[256,64]{0,1:T(8,128)(2,1)S(1)}, bf16[256,64]{0,1:T(8,128)(2,1)}, u32[]{:S(2)}) copy-start(bf16[256,64]{0,1:T(8,128)(2,1)} %param.23) | copy-start | bytes 98308
  116.2 2.7 copy-start.6
  119.0 3.1 copy-start.12
  121.2 8.2 %copy-start.13 = (bf16[256,512]{1,0:T(8,128)(2,1)S(1)}, bf16[256,512]{1,0:T(8,128)(2,1)}, u32[]{:S(2)}) copy-start(bf16[256,512]{1,0:T(8,128)(2,1)} %param.22) | copy-start | bytes 786436
  130.6 2.1 copy-start.11
  130.6 2.2 copy-start.10
  130.6 109.4 %all-gather.12.cloned.1.call-start = ((), (), s32[]{:S(2)}) async-start(), calls=%async_computation.2 | async-start | bytes 6488064 | tf_op jit(solution)/shard_map/all_gather | solution.py:188
  131.3 201.4 %all-gather.14.cloned.1.call-start = ((), (), s32[]{:S(2)}) async-start(), calls=%async_computation.3 | async-start | bytes 6488064 | tf_op jit(solution)/shard_map/all_gather | solution.py:189
  132.1 293.9 %all-gather.16.cloned.1.call-start = ((), (), s32[]{:S(2)}) async-start(), calls=%async_computation.4 | async-start | bytes 6488064 | tf_op jit(solution)/shard_map/all_gather | solution.py:202
  132.7 324.1 %reduce-scatter.2.cloned.1.call-start = ((), (), s32[]{:S(2)}) async-start(), calls=%async_computation.5 | async-start | bytes 1310720 | tf_op jit(solution)/shard_map/reduce_scatter | solution.py:205
  147.0 185.7 %copy-start.2 = (bf16[256,2048]{1,0:T(8,128)(2,1)S(1)}, bf16[256,2048]{1,0:T(8,128)(2,1)}, u32[]{:S(2)}) copy-start(bf16[256,2048]{1,0:T(8,128)(2,1)} %all-gather.10.cloned.1.call-done) | copy-start | bytes 3145732
  244.8 0.9 copy-start.3
  245.7 94.1 %collective-permute-start = (bf16[2,1408]{1,0:T(2,128)(2,1)S(1)}, bf16[2,1408]{1,0:T(2,128)(2,1)S(1)}, u32[]{:S(2)}, u32[]{:S(2)}) collective-permute-start(bf16[2,1408]{1,0:T(2,128)(2,1)S(1)} %slice.123), channel_id=1, source_target_pairs={{0,4},{4,8},{8,12},{12,16},{16,20},{20,24},{24,28},{1,5},{5,9},{9,... | collective-permute-start | bytes 16904 | tf_op jit(solution)/shard_map/ppermute | solution.py:38
  332.7 7.1 %copy-start.4 = (bf16[256,1408]{1,0:T(8,128)(2,1)S(1)}, bf16[256,1408]{1,0:T(8,128)(2,1)}, u32[]{:S(2)}) copy-start(bf16[256,1408]{1,0:T(8,128)(2,1)} %copy-done.3) | copy-start | bytes 2162692
  337.3 3.8 collective-permute-start.1
  426.0 30.8 %copy-start.1 = (bf16[256,512]{1,0:T(8,128)(2,1)S(1)}, bf16[256,512]{1,0:T(8,128)(2,1)}, u32[]{:S(2)}) copy-start(bf16[256,512]{1,0:T(8,128)(2,1)} %fusion.39) | copy-start | bytes 786436
Sparse Core Ops, SparseCore 0:
  130.7 14.7 all-gather.9
  147.7 92.3 all-gather.11
  242.2 90.4 all-gather.13
  334.6 91.3 all-gather.15
  433.8 22.9 reduce-scatter.1
where the time goes:
time: 465 us
  waiting for transfers between devices  300 us (65%)
  blocking collectives  108 us (23%)
  matrix products  23.7 us (5%)
  between operations  14.1 us (3%)
  other arithmetic  7.93 us (2%)
  local copies, waits for them, and re-layouts  5.9 us (1%)
  starting transfers between devices  5.07 us (1%)
    all_gather x1, waiting for transfers between devices, local(): lax.all_gather(switch_expansion_matrix, 'sp', axis=0, tiled=True)  93 us
    all_gather x1, waiting for transfers between devices, local(): lax.all_gather(content_expansion_matrix, 'sp', axis=0, tiled=True)  84.5 us
    all_gather x1, waiting for transfers between devices, local(): lax.all_gather(contraction_matrix, 'sp', axis=1, tiled=True)  83.6 us
    all_gather x3, blocking collectives, entering(): lax.all_gather(part.astype(kind), axis)  79.3 us
    reduce_scatter x1, waiting for transfers between devices, local(): lax.psum_scatter(terms.astype(jnp.bfloat16), 'tp', scatter_dimension=1, t...  23.1 us
    unnamed x1, blocking collectives  21.4 us
    all_gather x1, waiting for transfers between devices, local(): whole = lax.all_gather(resid, 'tp', axis=1, tiled=True).astype(jnp.float32)  12.6 us
  transfers between devices with their start and end apart: 7, of which 6 were waited for; matrix products, arithmetic and copies ran while one was open for 3% of the time, Pallas kernels for 0%

commit v1 on v0

--- a/solution.py
+++ b/solution.py
@@ -7,6 +7,11 @@
 EPSILON = 1e-06
 SOFTENING = 16.0
 HIGHEST = lax.Precision.HIGHEST
+
+
+def gathered_along(x, name, dim):
+    tiles = lax.all_gather(x, name)
+    return jnp.concatenate(tiles, axis=dim)
 
 
 def entering(value, axis, combine, identity):
@@ -198,9 +203,7 @@
     conv_gate = convolve(gate_ext, taps[:, 1])
     hidden = (jax.nn.silu(conv_gate) * conv_value).astype(jnp.bfloat16)
     terms = jnp.dot(
-        hidden,
-        lax.all_gather(contraction_matrix, "sp", axis=1, tiled=True),
-        preferred_element_type=jnp.float32,
+        hidden, gathered_along(contraction_matrix, "sp", 1), preferred_element_type=jnp.float32
     )
     down = lax.psum_scatter(
         terms.astype(jnp.bfloat16), "tp", scatter_dimension=1, tiled=True

time: 465 us -> 474 us (1.019)
  local copies, waits for them, and re-layouts: 5.9 us -> 15.1 us
    reshape x0 -> x1, local copies, waits for them, and re-layouts: none -> 8.3 us  [gathered_along(): return jnp.concatenate(tiles, axis=dim)]
  transfers between devices with their start and end apart: 7 -> 7, of which waited for: 6 -> 5; matrix products, arithmetic and copies ran while one was open for 3% -> 5% of each run, Pallas kernels for 0% -> 0%
where the time goes in v1:
time: 474 us; the launch traced here: 473 us
  waiting for transfers between devices  300 us (63%)
  blocking collectives  108 us (23%)
  matrix products  22.2 us (5%)
  local copies, waits for them, and re-layouts  15.1 us (3%)
  between operations  14.2 us (3%)
  other arithmetic  7.4 us (2%)
  starting transfers between devices  5.65 us (1%)
    all_gather x1, waiting for transfers between devices, local(): lax.all_gather(switch_expansion_matrix, 'sp', axis=0, tiled=True)  93 us
    all_gather x1, waiting for transfers between devices, gathered_along(): tiles = lax.all_gather(x, name)  85.6 us
    all_gather x1, waiting for transfers between devices, local(): lax.all_gather(content_expansion_matrix, 'sp', axis=0, tiled=True)  84.2 us
    all_gather x3, blocking collectives, entering(): lax.all_gather(part.astype(kind), axis)  79.3 us
    reduce_scatter x1, waiting for transfers between devices, local(): lax.psum_scatter(terms.astype(jnp.bfloat16), 'tp', scatter_dimension=1, t...  23.1 us
    unnamed x1, blocking collectives  21.4 us
    all_gather x1, waiting for transfers between devices, local(): whole = lax.all_gather(resid, 'tp', axis=1, tiled=True).astype(jnp.float32)  12 us
  transfers between devices with their start and end apart: 7, of which 5 were waited for; matrix products, arithmetic and copies ran while one was open for 5% of the time, Pallas kernels for 0%

profile of v1, /device:TPU:0, one launch (start us, length us, event | category | flops | bytes accessed | tf_op | source)
XLA Modules:
  0.0 472.8 jit_solution(8109465501970935813)
XLA Ops:
  6.6 1.3 fusion.88
  7.9 1.2 fusion.87
  9.1 0.7 fusion.89
  9.8 0.8 fusion.79
  11.1 0.3 fusion.43
  11.4 32.3 %all-gather.1 = bf16[512,128]{1,0:T(8,128)(2,1)S(1)} all-gather(bf16[64,128]{1,0:T(8,128)(2,1)S(1)} %fusion.43), channel_id=3, replica_groups=mesh['sp'=8,'tp'=4] {'sp'}, dimensions={0}, use_global_device_ids=true | all-gather | bytes 147456 | tf_op jit(solution)/shard_map/all_gather | solution.py:20
  44.1 0.3 fusion.42
  44.4 30.7 %all-gather.3 = bf16[1024,128]{1,0:T(8,128)(2,1)S(1)} all-gather(bf16[128,128]{1,0:T(8,128)(2,1)S(1)} %fusion.42), channel_id=5, replica_groups=mesh['sp'=8,'tp'=4] {'sp'}, dimensions={0}, use_global_device_ids=true | all-gather | bytes 294912 | tf_op jit(solution)/shard_map/all_gather | solution.py:20
  75.1 0.6 dynamic-slice
  76.7 21.4 %all-reduce = bf16[512]{0:T(512)(128)(2,1)S(1)} all-reduce(bf16[512]{0:T(512)(128)(2,1)S(1)} %dynamic-update-slice), channel_id=2, replica_groups=mesh['sp'=8,'tp'=4] {'sp'}, use_global_device_ids=true, to_apply=%add | all-reduce | flops 512 | bytes 2048
  98.1 16.3 %all-gather.5 = bf16[8,1,128]{2,1,0:T(2,128)(2,1)S(1)} all-gather(bf16[1,1,128]{2,1,0:T(2,128)(2,1)S(1)} %convert_bitcast_fusion), channel_id=4, replica_groups=mesh['sp'=8,'tp'=4] {'sp'}, dimensions={0}, use_global_device_ids=true | all-gather | bytes 2304 | tf_op jit(solution)/shard_map/all_gather | solution.py:20
  114.4 1.6 while.42
  116.2 1.8 while.40
  116.4 0.2 fusion.124
  116.9 0.2 fusion.124
  117.3 0.2 fusion.124
  117.8 0.2 fusion.124
  118.1 0.4 convolution_select_fusion.1
  118.4 0.3 multiply_reduce_fusion.1
  119.0 2.1 while.41
  119.3 0.3 fusion.131
  119.8 0.3 fusion.131
  120.3 0.3 fusion.131
  120.9 0.3 fusion.131
  121.2 0.4 convolution_select_fusion
  121.6 0.3 multiply_reduce_fusion
  122.2 7.2 %all_gather.44 = bf16[256,1024]{0,1:T(8,128)(2,1)S(1)} all-gather(bf16[256,256]{0,1:T(8,128)(2,1)S(1)} %bitcast.242), channel_id=1, replica_groups=mesh['sp'=8,'tp'=4] {'tp'}, dimensions={1}, use_global_device_ids=true | all-gather | bytes 655360 | tf_op jit(solution)/shard_map/all_gather | solution.py:181
  129.4 1.2 fusion.39
  130.6 0.7 all-gather.13.cloned.1.call-update
  131.4 0.7 all-gather.15.cloned.1.call-update
  132.1 0.5 all-gather.17.cloned.1.call-update
  132.7 0.7 slice_reduce_fusion.5
  133.4 12.0 %all-gather.11.cloned.1.call-done = bf16[256,2048]{1,0:T(8,128)(2,1)} async-done(((bf16[256,512]{1,0:T(8,128)(2,1)}), bf16[256,2048]{1,0:T(8,128)(2,1)}) %all-gather.11.cloned.1.call-update) | async-done | bytes 1048592 | tf_op jit(solution)/shard_map/all_gather | solution.py:189
  145.5 1.5 fusion.30
  147.0 93.0 %all-gather.13.cloned.1.call-done = bf16[2048,1408]{1,0:T(8,128)(2,1)} async-done(((bf16[256,1408]{1,0:T(8,128)(2,1)}), bf16[2048,1408]{1,0:T(8,128)(2,1)}) %all-gather.13.cloned.1.call-update) | async-done | bytes 5767184 | tf_op jit(solution)/shard_map/all_gather | solution.py:193
  240.0 4.8 %convolution_convert_fusion.1 = bf16[256,1408]{1,0:T(8,128)(2,1)S(1)} fusion(bf16[2048,1408]{1,0:T(8,128)(2,1)} %all-gather.13.cloned.1.call-done, bf16[256,2048]{1,0:T(8,128)(2,1)} %all-gather.11.cloned.1.call-done, f32[2048]{0:T(1024)S(1)} %convert_element_type.216, f32[256]{0:T(256)S(1)} %add_rsqrt_fusion.2), kind=kOutput, calls=%fused_computation.43 | convolution fusion | flops 1478852608 | bytes 7545856 | tf_op jit(solution)/shard_map/dot_general | solution.py:196
  244.8 0.6 slice.123
  245.4 3.0 collective-permute-start
  248.5 84.2 %all-gather.15.cloned.1.call-done = bf16[2048,1408]{1,0:T(8,128)(2,1)} async-done(((bf16[256,1408]{1,0:T(8,128)(2,1)}), bf16[2048,1408]{1,0:T(8,128)(2,1)}) %all-gather.15.cloned.1.call-update) | async-done | bytes 5767184 | tf_op jit(solution)/shard_map/all_gather | solution.py:194
  332.7 4.5 convolution_convert_fusion
  337.2 2.5 collective-permute-start.1
  339.7 85.6 %all-gather.17.cloned.1.call-done = bf16[11264,256]{1,0:T(8,128)(2,1)} async-done(((bf16[1408,256]{1,0:T(8,128)(2,1)}), bf16[11264,256]{1,0:T(8,128)(2,1)}) %all-gather.17.cloned.1.call-update) | async-done | bytes 5767184 | tf_op jit(solution)/shard_map/all_gather | solution.py:13
  425.3 8.3 %copy.85 = bf16[1408,8,256]{0,2,1:T(8,128)(2,1)} copy(bf16[1408,8,256]{2,0,1:T(8,128)(2,1)} %bitcast.221) | data formatting | bytes 11534336 | tf_op jit(solution)/shard_map/reshape | solution.py:14
  433.6 0.8 maximum_convert_fusion
  434.6 0.5 copy-done.9
  435.2 6.3 %convolution_convert_fusion.2 = bf16[256,2048]{1,0:T(8,128)(2,1)} fusion(bf16[1408,2048]{0,1:T(8,128)(2,1)} %bitcast.222, f32[258,1408]{1,0:T(8,128)S(1)} %maximum_convert_fusion.1, f32[258,1408]{1,0:T(8,128)S(1)} %maximum_convert_fusion, f32[1408]{0:T(1024)S(1)} %copy-done.9, f32[1408]{0:T(1024)S(1)} %copy-done.10, f32[1408]{0:T(1024)S(1)} %copy-done.11, ...), kind=kOutput, calls=%fused_computation.44 | convolution fusion | flops 1482686464 | bytes 15515648 | tf_op jit(solution)/shard_map/dot_general | solution.py:205
  441.5 23.1 %reduce-scatter.2.cloned.1.call-done = bf16[256,512]{1,0:T(8,128)(2,1)} async-done(((bf16[256,2048]{1,0:T(8,128)(2,1)}), bf16[256,512]{1,0:T(8,128)(2,1)}) %reduce-scatter.2.cloned.1.call-update) | async-done | bytes 262160 | tf_op jit(solution)/shard_map/reduce_scatter | solution.py:208
  464.6 1.7 add_convert_fusion
  (137 shorter events, 5.3 us)
Async XLA Ops:
  6.5 122.8 %copy-start = (bf16[1024,512]{1,0:T(8,128)(2,1)S(1)}, bf16[1024,512]{1,0:T(8,128)(2,1)}, u32[]{:S(2)}) copy-start(bf16[1024,512]{1,0:T(8,128)(2,1)} %param.32) | copy-start | bytes 3145732
  6.5 4.4 copy-start.6
  6.5 37.2 %copy-start.3 = (bf16[256,128]{1,0:T(8,128)(2,1)S(1)}, bf16[256,128]{1,0:T(8,128)(2,1)}, u32[]{:S(2)}) copy-start(bf16[256,128]{1,0:T(8,128)(2,1)} %param.28) | copy-start | bytes 196612
  6.5 138.9 %all-gather.11.cloned.1.call-start = ((), (), s32[]{:S(2)}) async-start(), calls=%async_computation.1 | async-start | bytes 1310720 | tf_op jit(solution)/shard_map/all_gather | solution.py:189
  6.6 37.5 %copy-start.4 = (bf16[256,128]{1,0:T(8,128)(2,1)S(1)}, bf16[256,128]{1,0:T(8,128)(2,1)}, u32[]{:S(2)}) copy-start(bf16[256,128]{1,0:T(8,128)(2,1)} %param.27) | copy-start | bytes 196612
  9.8 65.3 %copy-start.18 = (u32[32]{0:T(128)S(1)}, u32[32]{0:T(128)}, u32[]{:S(2)}) copy-start(u32[32]{0:T(128)} %constant.109) | copy-start | bytes 388
  43.7 72.3 %copy-start.7 = (bf16[256,64]{0,1:T(8,128)(2,1)S(1)}, bf16[256,64]{0,1:T(8,128)(2,1)}, u32[]{:S(2)}) copy-start(bf16[256,64]{0,1:T(8,128)(2,1)} %param.23) | copy-start | bytes 98308
  116.2 2.7 copy-start.5
  119.0 3.0 copy-start.15
  121.2 8.2 %copy-start.17 = (bf16[256,512]{1,0:T(8,128)(2,1)S(1)}, bf16[256,512]{1,0:T(8,128)(2,1)}, u32[]{:S(2)}) copy-start(bf16[256,512]{1,0:T(8,128)(2,1)} %param.22) | copy-start | bytes 786436
  130.5 2.1 copy-start.14
  130.5 2.2 copy-start.8
  130.6 109.4 %all-gather.13.cloned.1.call-start = ((), (), s32[]{:S(2)}) async-start(), calls=%async_computation.2 | async-start | bytes 6488064 | tf_op jit(solution)/shard_map/all_gather | solution.py:193
  131.3 201.4 %all-gather.15.cloned.1.call-start = ((), (), s32[]{:S(2)}) async-start(), calls=%async_computation.3 | async-start | bytes 6488064 | tf_op jit(solution)/shard_map/all_gather | solution.py:194
  132.1 293.2 %all-gather.17.cloned.1.call-start = ((), (), s32[]{:S(2)}) async-start(), calls=%async_computation.5 | async-start | bytes 6488064 | tf_op jit(solution)/shard_map/all_gather | solution.py:13
  132.6 331.9 %reduce-scatter.2.cloned.1.call-start = ((), (), s32[]{:S(2)}) async-start(), calls=%async_computation.4 | async-start | bytes 1310720 | tf_op jit(solution)/shard_map/reduce_scatter | solution.py:208
  147.0 97.8 %copy-start.16 = (f32[256]{0:T(256)}, f32[256]{0:T(256)S(1)}, u32[]{:S(2)}) copy-start(f32[256]{0:T(256)S(1)} %add_rsqrt_fusion.2) | copy-start | bytes 3076
  147.0 185.7 %copy-start.2 = (bf16[256,2048]{1,0:T(8,128)(2,1)S(1)}, bf16[256,2048]{1,0:T(8,128)(2,1)}, u32[]{:S(2)}) copy-start(bf16[256,2048]{1,0:T(8,128)(2,1)} %all-gather.11.cloned.1.call-done) | copy-start | bytes 3145732
  245.4 188.1 %collective-permute-start = (bf16[2,1408]{1,0:T(2,128)(2,1)}, bf16[2,1408]{1,0:T(2,128)(2,1)}, u32[]{:S(2)}, u32[]{:S(2)}) collective-permute-start(bf16[2,1408]{1,0:T(2,128)(2,1)} %slice.123), channel_id=1, source_target_pairs={{0,4},{4,8},{8,12},{12,16},{16,20},{20,24},{24,28},{1,5},{5,9},{9,... | collective-permute-start | bytes 16904 | tf_op jit(solution)/shard_map/ppermute | solution.py:43
  337.2 97.2 %collective-permute-start.1 = (bf16[2,1408]{1,0:T(2,128)(2,1)S(1)}, bf16[2,1408]{1,0:T(2,128)(2,1)S(1)}, u32[]{:S(2)}, u32[]{:S(2)}) collective-permute-start(bf16[2,1408]{1,0:T(2,128)(2,1)S(1)} %slice.130), channel_id=1, source_target_pairs={{0,4},{4,8},{8,12},{12,16},{16,20},{20,24},{24,28},{1,5},{5,9},{9,... | collective-permute-start | bytes 16904 | tf_op jit(solution)/shard_map/ppermute | solution.py:43
  434.4 0.7 copy-start.9
  434.4 0.7 copy-start.10
  434.4 0.7 copy-start.11
  434.4 0.7 copy-start.12
  434.5 0.7 copy-start.13
  435.2 29.4 %copy-start.1 = (bf16[256,512]{1,0:T(8,128)(2,1)S(1)}, bf16[256,512]{1,0:T(8,128)(2,1)}, u32[]{:S(2)}) copy-start(bf16[256,512]{1,0:T(8,128)(2,1)} %fusion.39) | copy-start | bytes 786436
Sparse Core Ops, SparseCore 0:
  130.7 14.7 all-gather.10
  147.6 92.3 all-gather.12
  242.2 90.4 all-gather.14
  334.7 90.4 all-gather.16
  441.6 22.9 reduce-scatter.1
